TPU v7x, 32 devices: a whole 2x2x4 slice. The times are simulated.
32 devices in a mesh: kv: 8 (over z, x), tp: 4 (over y, core).
Axes of the slice: x: 2, y: 2, z: 4, core: 2. Of those that a mesh axis runs over, the one named last changes fastest.
Arguments:
- hidden_rows: bfloat16 [28, 4096], P(None, ('kv', 'tp')), may hold values from -6 to 6
- first_gain: float32 [4096], P('kv'), may hold values from 0.1 to 1.9
- first_gate: bfloat16 [4096, 11264], P('kv', 'tp'), may hold values from -0.125 to 0.125
- first_up: bfloat16 [4096, 11264], P('kv', 'tp'), may hold values from -0.125 to 0.125
- first_down: bfloat16 [11264, 4096], P('tp', 'kv'), may hold values from -0.078125 to 0.078125
- mix_gain: float32 [4096], P('kv'), may hold values from 0.1 to 1.9
- query_weight: bfloat16 [4096, 2048], P('kv', 'tp'), may hold values from -0.09375 to 0.09375
- key_weight: bfloat16 [4096, 2048], P('kv', 'tp'), may hold values from -0.09375 to 0.09375
- value_weight: bfloat16 [4096, 2048], P('kv', 'tp'), may hold values from -0.09375 to 0.09375
- forget_weight: bfloat16 [4096, 16], P('kv'), may hold values from -0.09375 to 0.09375
- forget_bias: float32 [16], replicated, may hold values from -8 to 2
- out_weight: bfloat16 [2048, 4096], P('tp', 'kv'), may hold values from -0.5 to 0.5
- second_gain: float32 [4096], P('kv'), may hold values from 0.1 to 1.9
- second_gate: bfloat16 [4096, 11264], P('kv', 'tp'), may hold values from -0.125 to 0.125
- second_up: bfloat16 [4096, 11264], P('kv', 'tp'), may hold values from -0.125 to 0.125
- second_down: bfloat16 [11264, 4096], P('tp', 'kv'), may hold values from -0.078125 to 0.078125
- cache_keys: bfloat16 [28, 2048, 2048], P(None, 'kv', 'tp'), may hold values from -48 to 48
- cache_values: bfloat16 [28, 2048, 2048], P(None, 'kv', 'tp'), may hold values from -6 to 6
- cache_gates: float32 [28, 16, 2048], P(None, 'tp', 'kv'), may hold values from -1 to 0
- lengths: int32 [28], replicated, may hold values from 1 to 2048, 16384 in all
Outputs:
- out_rows: bfloat16 [28, 4096], P(None, ('kv', 'tp'))
Inputs may be any that keep to these rules, and one draw needn't show every extreme that they name: Sequence b uses cache positions 0 to lengths[b] - 1; some sequence uses all 2048.
All inputs are finite; a program needn't handle non-finite values.
Results may differ from a plain program's by a relative error of at most 0.014.
Values may be sent and summed in bfloat16 or wider, within the bound.
A program may use at most 128 MiB of HBM per device.

v0:
```python
import jax
import jax.numpy as jnp
from jax import lax
from jax.sharding import PartitionSpec as P

D = 4096
HEAD_DIM = 128


EPS = 1e-06
FLOOR = -1e30


def entering(x, axis, combine, identity):
    devices, mine = (lax.axis_size(axis), lax.axis_index(axis))
    everything = lax.all_gather(x, axis)
    start = jnp.broadcast_to(jnp.asarray(identity, x.dtype), x.shape)

    def lap(k, before):
        reached = k < mine
        new = combine(before, everything[k])
        return jnp.where(reached, new, before)

    return lax.fori_loop(0, devices, lap, start)


def joined(value, axis, join):
    pieces = jax.tree.map(lambda part: lax.all_gather(part, axis), value)
    head = jax.tree.map(lambda part: part[0], pieces)
    tail = jax.tree.map(lambda part: part[1:], pieces)
    total, _ = lax.scan(lambda total, share: (join(total, share), None), head, tail)
    return total


def widen(shard):
    return lax.all_gather(shard, "tp", axis=1, tiled=True)


def scaled_rows(block, gain):
    block32 = block.astype(jnp.float32)
    scaled = (block32 * gain).astype(jnp.bfloat16)
    squares = jnp.sum(block32 * block32, axis=1, keepdims=True)
    return (scaled, squares)


def feed_forward(block, gain, w_gate, w_up, w_down):
    scaled, squares = scaled_rows(block, gain)
    gate = jnp.dot(scaled, w_gate, preferred_element_type=jnp.float32)
    up_act = jnp.dot(scaled, w_up, preferred_element_type=jnp.float32)
    gate, up_act, squares = lax.psum((gate, up_act, squares), "kv")
    rscale = lax.rsqrt(squares / D + EPS)
    hidden = (jax.nn.silu(gate * rscale) * (up_act * rscale)).astype(jnp.bfloat16)
    return jnp.dot(hidden, w_down, preferred_element_type=jnp.float32)


def join_parts(first, second):
    top_a, mass_a, summed_a = first
    top_b, mass_b, summed_b = second
    peak = jnp.maximum(top_a, top_b)
    part_a = jnp.exp(top_a - peak)
    part_b = jnp.exp(top_b - peak)
    return (
        peak,
        mass_a * part_a + mass_b * part_b,
        summed_a * part_a[:, :, None] + summed_b * part_b[:, :, None],
    )


def attention(
    block,
    gain,
    query_weight,
    key_weight,
    value_weight,
    forget_weight,
    forget_bias,
    out_weight,
    cache_keys,
    cache_values,
    cache_gates,
    lengths,
):
    scaled, squares = scaled_rows(block, gain)
    seqs = block.shape[0]
    heads_dev = query_weight.shape[1] // HEAD_DIM
    span = cache_keys.shape[1]
    places = lax.axis_index("kv") * span + jnp.arange(span, dtype=jnp.int32)
    live = places[None, None, :] < lengths[:, None, None]
    kept = jnp.where(live, cache_gates, 0.0)
    running = jnp.cumsum(kept, axis=2)
    local_total = running[:, :, -1:]
    lower = entering(local_total, "kv", jnp.add, jnp.zeros_like(local_total))
    part_query = jnp.dot(scaled, query_weight, preferred_element_type=jnp.float32)
    part_key = jnp.dot(scaled, key_weight, preferred_element_type=jnp.float32)
    part_value = jnp.dot(scaled, value_weight, preferred_element_type=jnp.float32)
    part_logit = jnp.dot(scaled, forget_weight, preferred_element_type=jnp.float32)
    part_query, part_key, part_value, part_logit, squares, grand = lax.psum(
        (part_query, part_key, part_value, part_logit, squares, local_total), "kv"
    )
    rscale = lax.rsqrt(squares / D + EPS)
    query = (part_query * rscale).astype(jnp.bfloat16).reshape(seqs, heads_dev, HEAD_DIM)
    fresh_key = (part_key * rscale).astype(jnp.bfloat16).reshape(seqs, heads_dev, HEAD_DIM)
    fresh_value = (part_value * rscale).astype(jnp.bfloat16).reshape(seqs, heads_dev, HEAD_DIM)
    first_head = lax.axis_index("tp") * heads_dev
    own_logit = lax.dynamic_slice_in_dim(part_logit, first_head, heads_dev, 1)
    own_bias = lax.dynamic_slice_in_dim(forget_bias, first_head, heads_dev, 0)
    fresh_gate = jax.nn.log_sigmoid(own_logit * rscale + own_bias)
    bias = fresh_gate[:, :, None] + (grand - lower - running)
    factor = HEAD_DIM ** (-0.5)
    keys = cache_keys.reshape(seqs, span, heads_dev, HEAD_DIM)
    values = cache_values.reshape(seqs, span, heads_dev, HEAD_DIM)
    scores = (
        jnp.einsum("bphd,bhd->bhp", keys, query, preferred_element_type=jnp.float32) * factor + bias
    )
    top = jnp.max(jnp.where(live, scores, FLOOR), axis=2)
    weights = jnp.where(live, jnp.exp(scores - top[:, :, None]), 0.0)
    mass = jnp.sum(weights, axis=2)
    summed = jnp.einsum(
        "bhp,bphd->bhd", weights.astype(jnp.bfloat16), values, preferred_element_type=jnp.float32
    )
    top, mass, summed = joined((top, mass, summed), "kv", join_parts)
    own = jnp.einsum("bhd,bhd->bh", query, fresh_key, preferred_element_type=jnp.float32) * factor
    peak = jnp.maximum(top, own)
    keep = jnp.exp(top - peak)
    fresh = jnp.exp(own - peak)
    attended = (
        (summed * keep[:, :, None] + fresh_value.astype(jnp.float32) * fresh[:, :, None])
        / (mass * keep + fresh)[:, :, None]
    ).astype(jnp.bfloat16)
    attended = attended.reshape(seqs, heads_dev * HEAD_DIM)
    return jnp.dot(attended, out_weight, preferred_element_type=jnp.float32)


def advance(shard, block, partial_value, weight):
    total = lax.psum(partial_value, "tp")
    return (shard, (block.astype(jnp.float32) + weight * total).astype(jnp.bfloat16))


def local(
    hidden_rows,
    first_gain,
    first_gate,
    first_up,
    first_down,
    mix_gain,
    query_weight,
    key_weight,
    value_weight,
    forget_weight,
    forget_bias,
    out_weight,
    second_gain,
    second_gate,
    second_up,
    second_down,
    cache_keys,
    cache_values,
    cache_gates,
    lengths,
):
    shard = hidden_rows
    block = widen(shard)
    partial_value = feed_forward(block, first_gain, first_gate, first_up, first_down)
    shard, block = advance(shard, block, partial_value, 0.5)
    partial_value = attention(
        block,
        mix_gain,
        query_weight,
        key_weight,
        value_weight,
        forget_weight,
        forget_bias,
        out_weight,
        cache_keys,
        cache_values,
        cache_gates,
        lengths,
    )
    shard, block = advance(shard, block, partial_value, 1.0)
    partial_value = feed_forward(block, second_gain, second_gate, second_up, second_down)
    shard, block = advance(shard, block, partial_value, 0.5)
    columns = hidden_rows.shape[1]
    return lax.dynamic_slice_in_dim(block, lax.axis_index("tp") * columns, columns, 1)


def solution(mesh):
    return jax.shard_map(
        local,
        mesh=mesh,
        in_specs=(
            P(None, ("kv", "tp")),
            P("kv"),
            P("kv", "tp"),
            P("kv", "tp"),
            P("tp", "kv"),
            P("kv"),
            P("kv", "tp"),
            P("kv", "tp"),
            P("kv", "tp"),
            P("kv", None),
            P(),
            P("tp", "kv"),
            P("kv"),
            P("kv", "tp"),
            P("kv", "tp"),
            P("tp", "kv"),
            P(None, "kv", "tp"),
            P(None, "kv", "tp"),
            P(None, "tp", "kv"),
            P(),
        ),
        out_specs=P(None, ("kv", "tp")),
        check_vma=False,
    )
```

profile of v0, /device:TPU:0, one launch (start us, length us, event | category | flops | bytes accessed | tf_op | source)
XLA Modules:
  0.0 400.4 jit_solution(7020302194779085242)
XLA Ops:
  6.5 6.5 %all_gather.27 = bf16[28,512]{1,0:T(8,128)(2,1)S(1)} all-gather(bf16[28,128]{1,0:T(8,128)(2,1)} %param.24), channel_id=1, replica_groups=mesh['kv'=8,'tp'=4] {'tp'}, dimensions={1}, use_global_device_ids=true | all-gather | bytes 35840 | tf_op jit(solution)/shard_map/all_gather | solution.py:36
  13.1 2.0 fusion.27
  15.1 1.3 fusion.29
  16.8 2.3 reduce-window.6
  20.8 31.5 %all-gather = f32[224,4,1]{1,2,0:T(1,128)S(1)} all-gather(f32[28,4,1]{1,2,0:T(1,128)S(1)} %copy.78), channel_id=2, replica_groups=mesh['kv'=8,'tp'=4] {'kv'}, dimensions={0}, use_global_device_ids=true | all-gather | bytes 4032 | tf_op jit(solution)/shard_map/all_gather | solution.py:16
  52.6 21.3 %psum.106 = f32[28,1]{0,1:T(1,128)S(1)} all-reduce(f32[28,1]{0,1:T(1,128)S(1)} %bitcast.89), channel_id=1, replica_groups=mesh['kv'=8,'tp'=4] {'kv'}, use_global_device_ids=true, to_apply=%region_2.0 | all-reduce | flops 28 | bytes 224 | tf_op jit(solution)/shard_map/psum | solution.py:50
  73.9 19.2 %all-reduce.11.cloned.1.call-done = (f32[28,2816]{1,0:T(8,128)}, f32[28,2816]{1,0:T(8,128)}) async-done(((f32[28,2816]{1,0:T(8,128)}, f32[28,2816]{1,0:T(8,128)}), (f32[28,2816]{1,0:T(8,128)}, f32[28,2816]{1,0:T(8,128)})) %all-reduce.11.cloned.1.call-update) | async-done | bytes 630800 | tf_op jit(solution)/shard_map/psum | solution.py:50
  93.1 2.7 fusion.6
  95.8 10.7 %psum.108 = f32[28,512]{1,0:T(8,128)S(1)} all-reduce(f32[28,512]{1,0:T(8,128)S(1)} %fusion.6), channel_id=1, replica_groups=mesh['kv'=8,'tp'=4] {'tp'}, use_global_device_ids=true, to_apply=%region_4.5 | all-reduce | flops 14336 | bytes 114688 | tf_op jit(solution)/shard_map/psum | solution.py:135
  107.2 0.7 fusion.35
  107.9 1.9 fusion.33
  109.8 1.9 fusion.31
  111.6 1.9 fusion.37
  114.0 10.4 %copy.97 = bf16[28,256,512]{1,2,0:T(8,128)(2,1)} copy(bf16[28,256,512]{2,1,0:T(8,128)(2,1)} %param.40) | data formatting | bytes 14680064 | tf_op jit(solution)/shard_map/reshape | solution.py:110
  124.5 60.4 %all-reduce.7.cloned.1.call-done = (f32[28,512]{1,0:T(8,128)}, f32[28,1]{0,1:T(1,128)}, f32[28,512]{1,0:T(8,128)}, f32[28,4,1]{0,1,2:T(4,128)}, f32[28,16]{0,1:T(8,128)}, /*index=5*/f32[28,512]{1,0:T(8,128)}) async-done(((f32[28,512]{1,0:T(8,128)}, f32[28,1]{0,1:T(1,128)}, f32[28,512]{1,0:T(8,128)}, f32[28,4,1]{0,1,2:T(4,128)}, f32[28,16]{0,1:T(8,128)}, /*index=5*/f32[28,512]{1,0:T(8,128)}), ...) | async-done | bytes 174400 | tf_op jit(solution)/shard_map/psum | solution.py:97
  185.5 1.0 multiply_convert_fusion.6
  186.6 0.8 fusion.44
  188.2 4.1 %fusion.54 = f32[28,4,1,256]{3,2,1,0:T(1,128)S(1)} fusion(bf16[28,4,128,1]{2,3,1,0:T(2,128)(2,1)S(1)} %reshape.110, bf16[28,256,4,128]{1,3,2,0:T(8,128)(2,1)} %bitcast.79), kind=kOutput, calls=%fused_computation.84 | convolution fusion | flops 7340032 | bytes 7483392 | tf_op jit(solution)/shard_map/bphd,bhd->bhp/dot_general | solution.py:113
  193.0 26.1 %all-gather.5 = f32[8,28,4]{1,2,0:T(4,128)S(1)} all-gather(f32[1,28,4]{1,2,0:T(4,128)S(1)} %bitcast.86), channel_id=4, replica_groups=mesh['kv'=8,'tp'=4] {'kv'}, dimensions={0}, use_global_device_ids=true | all-gather | bytes 4032 | tf_op jit(solution)/shard_map/all_gather | solution.py:28
  219.7 26.1 %all-gather.4 = f32[8,28,4]{1,2,0:T(4,128)S(1)} all-gather(f32[1,28,4]{1,2,0:T(4,128)S(1)} %bitcast.85), channel_id=3, replica_groups=mesh['kv'=8,'tp'=4] {'kv'}, dimensions={0}, use_global_device_ids=true | all-gather | bytes 4032 | tf_op jit(solution)/shard_map/all_gather | solution.py:28
  246.4 4.1 %fusion.3 = f32[28,4,1,128]{3,2,1,0:T(1,128)S(1)} fusion(bf16[28,4,256,1]{2,1,0,3:T(4,128)(2,1)S(1)} %get-tuple-element.207, bf16[28,256,512]{2,1,0:T(8,128)(2,1)} %param.41), kind=kOutput, calls=%fused_computation.10 | convolution fusion | flops 7340032 | bytes 7454720 | tf_op jit(solution)/shard_map/bhp,bphd->bhd/dot_general | solution.py:118
  250.6 31.3 %all-gather.3 = f32[224,4,128]{2,1,0:T(4,128)S(1)} all-gather(f32[28,4,128]{2,1,0:T(4,128)S(1)} %bitcast.84), channel_id=5, replica_groups=mesh['kv'=8,'tp'=4] {'kv'}, dimensions={0}, use_global_device_ids=true | all-gather | bytes 516096 | tf_op jit(solution)/shard_map/all_gather | solution.py:28
  282.2 7.9 %while.28 = (s32[]{:T(128)}, f32[28,4]{0,1:T(4,128)S(1)}, f32[28,4]{0,1:T(4,128)S(1)}, f32[28,4,128]{2,1,0:T(4,128)S(1)}, f32[7,28,4]{1,2,0:T(4,128)}, /*index=5...) while((s32[]{:T(128)}, f32[28,4]{0,1:T(4,128)S(1)}, f32[28,4]{0,1:T(4,128)S(1)}, ...), condition=%wide.region_17.18_spmd, body=%wide.region_16.17_spmd.sunk | while | flops 43682 | bytes 178405 | solution.py:31
  282.2 0.7 fusion.74
  290.6 1.2 fusion.55
  291.8 10.7 %psum.115 = f32[28,512]{1,0:T(8,128)S(1)} all-reduce(f32[28,512]{1,0:T(8,128)S(1)} %fusion.55), channel_id=1, replica_groups=mesh['kv'=8,'tp'=4] {'tp'}, use_global_device_ids=true, to_apply=%region_20.21 | all-reduce | flops 14336 | bytes 114688 | tf_op jit(solution)/shard_map/psum | solution.py:135
  302.6 3.3 fusion.40
  305.9 1.3 fusion.41
  307.3 17.5 %psum.117 = f32[28,1]{0,1:T(1,128)S(1)} all-reduce(f32[28,1]{0,1:T(1,128)S(1)} %bitcast.88), channel_id=1, replica_groups=mesh['kv'=8,'tp'=4] {'kv'}, use_global_device_ids=true, to_apply=%region_23.24 | all-reduce | flops 28 | bytes 224 | tf_op jit(solution)/shard_map/psum | solution.py:50
  324.8 55.1 %all-reduce.9.cloned.1.call-done = (f32[28,2816]{1,0:T(8,128)}, f32[28,2816]{1,0:T(8,128)}) async-done(((f32[28,2816]{1,0:T(8,128)}, f32[28,2816]{1,0:T(8,128)}), (f32[28,2816]{1,0:T(8,128)}, f32[28,2816]{1,0:T(8,128)})) %all-reduce.9.cloned.1.call-update) | async-done | bytes 630800 | tf_op jit(solution)/shard_map/psum | solution.py:50
  379.9 2.7 fusion.7
  382.6 10.7 %psum.119 = f32[28,512]{1,0:T(8,128)S(1)} all-reduce(f32[28,512]{1,0:T(8,128)S(1)} %fusion.7), channel_id=1, replica_groups=mesh['kv'=8,'tp'=4] {'tp'}, use_global_device_ids=true, to_apply=%region_25.26 | all-reduce | flops 14336 | bytes 114688 | tf_op jit(solution)/shard_map/psum | solution.py:135
  (121 shorter events, 15.6 us)
Async XLA Ops:
  6.5 6.5 %copy-start = (bf16[512,2816]{1,0:T(8,128)(2,1)S(1)}, bf16[512,2816]{1,0:T(8,128)(2,1)}, u32[]{:S(2)}) copy-start(bf16[512,2816]{1,0:T(8,128)(2,1)} %param.27) | copy-start | bytes 8650756
  6.5 8.6 %copy-start.6 = (f32[512]{0:T(512)S(1)}, f32[512]{0:T(512)}, u32[]{:S(2)}) copy-start(f32[512]{0:T(512)} %param.25) | copy-start | bytes 6148
  6.5 86.6 %all-reduce.11.cloned.1.call-start = ((), (), s32[]{:S(2)}) async-start(), calls=%async_computation.2 | async-start | bytes 1441792 | tf_op jit(solution)/shard_map/psum | solution.py:50
  6.5 8.6 %copy-start.1 = (bf16[512,2816]{1,0:T(8,128)(2,1)S(1)}, bf16[512,2816]{1,0:T(8,128)(2,1)}, u32[]{:S(2)}) copy-start(bf16[512,2816]{1,0:T(8,128)(2,1)} %param.26) | copy-start | bytes 8650756
  13.1 3.5 copy-start.8
  13.1 3.6 copy-start.3
  16.5 168.4 %all-reduce.7.cloned.1.call-start = ((), (), s32[]{:S(2)}) async-start(), calls=%async_computation | async-start | bytes 414720 | tf_op jit(solution)/shard_map/psum | solution.py:97
  16.8 90.4 %copy-start.4 = (f32[512]{0:T(512)S(1)}, f32[512]{0:T(512)}, u32[]{:S(2)}) copy-start(f32[512]{0:T(512)} %param.29) | copy-start | bytes 6148
  16.8 90.4 %copy-start.5 = (bf16[512,16]{0,1:T(8,128)(2,1)S(1)}, bf16[512,16]{0,1:T(8,128)(2,1)}, u32[]{:S(2)}) copy-start(bf16[512,16]{0,1:T(8,128)(2,1)} %param.33) | copy-start | bytes 49156
  113.5 266.4 %all-reduce.9.cloned.1.call-start = ((), (), s32[]{:S(2)}) async-start(), calls=%async_computation.1 | async-start | bytes 1441792 | tf_op jit(solution)/shard_map/psum | solution.py:50
  114.0 10.4 %copy-start.9 = (f32[16]{0:T(128)S(1)}, f32[16]{0:T(128)}, u32[]{:S(2)}) copy-start(f32[16]{0:T(128)} %param.34) | copy-start | bytes 196
  250.6 52.1 %copy-start.7 = (f32[512]{0:T(512)S(1)}, f32[512]{0:T(512)}, u32[]{:S(2)}) copy-start(f32[512]{0:T(512)} %param.36) | copy-start | bytes 6148
  302.5 3.4 copy-start.2
Sparse Core Ops, SparseCore 0:
  16.6 76.4 all-reduce.10
  113.6 71.1 all-reduce.6
  307.4 72.4 all-reduce.8
where the time goes:
time: 401 us; the launch traced here: 400 us
  blocking collectives  192 us (48%)
  waiting for transfers between devices  135 us (34%)
  matrix products  29.2 us (7%)
  local copies, waits for them, and re-layouts  15.8 us (4%)
  other arithmetic  14.4 us (4%)
  between operations  13.4 us (3%)
    all_gather x3, blocking collectives, joined(): pieces = jax.tree.map(lambda part: lax.all_gather(part, axis), value)  83.5 us
    psum x2, waiting for transfers between devices, feed_forward(): gate, up_act, squares = lax.psum((gate, up_act, squares), 'kv')  74.3 us
    psum x1, waiting for transfers between devices, attention(): lax.psum((part_query, part_key, part_value, part_logit, squares, local_to...  60.4 us
    psum x2, blocking collectives, feed_forward(): gate, up_act, squares = lax.psum((gate, up_act, squares), 'kv')  38.8 us
    psum x3, blocking collectives, advance(): total = lax.psum(partial_value, 'tp')  32 us
    all_gather x1, blocking collectives, entering(): everything = lax.all_gather(x, axis)  31.5 us
    reshape x1, local copies, waits for them, and re-layouts, attention(): keys = cache_keys.reshape(seqs, span, heads_dev, HEAD_DIM)  10.4 us
  transfers between devices with their start and end apart: 3, of which 3 were waited for; matrix products, arithmetic and copies ran while one was open for 4% of the time, Pallas kernels for 0%

commit v1 on v0

v1 whole, which is shorter than its diff:
```python
import functools

import jax
import jax.numpy as jnp
from jax import lax
from jax.experimental import pallas as pl
from jax.experimental.pallas import tpu as pltpu
from jax.sharding import PartitionSpec as P

HEAD_DIM = 128
LANES = 128
SUB = 8
EPS = 1e-06
FLOOR = -1e30
MESH = pl.DeviceIdType.MESH
F32 = jnp.float32
BF16 = jnp.bfloat16

RS1, AG1, RSQ, AGQ, RSA, AGA, RS2, AG2 = range(8)
GATHER, SUM1, SUM2, SUM3 = range(4)


def up_to(value, step):
    return -(-value // step) * step


def hi_lo(column, rows):
    lane = lax.broadcasted_iota(jnp.int32, (rows, LANES), 1)
    wide = jnp.broadcast_to(column, (rows, LANES))
    hi = wide.astype(BF16).astype(F32)
    return jnp.where(lane < LANES // 2, hi, wide - hi).astype(BF16)


def from_hi_lo(tile):
    return tile[:, 0:1] + tile[:, LANES // 2 : LANES // 2 + 1]


def dot(a, b):
    return jnp.dot(a, b, preferred_element_type=F32)


def kernel(
    c,
    hid, g1, gm, g2, fw, cg, fb, lens,
    wg1, wu1, wd1, wq, wk, wv, wo, wg2, wu2, wd2, ck, cv,
    out,
    wg1_v, wu1_v, wd1_v, wq_v, wk_v, wv_v, wo_v, wg2_v, wu2_v, wd2_v, ck_v, cv_v,
    xg, rs_send1, rs_recv1, hid1, sum1_send, sum1,
    q_send, q_recv, q_buf, q_all, fwx, gpad, bias, total, sc, pv, stat, a_send, a_recv, att, att_all,
    sum2_send, sum2, rs_send2, rs_recv2, hid2, fin_send, fin_recv, fin_x, rows,
    ld_sem, kv_send, kv_recv, tp_send, tp_recv,
):
    K, T, R, RP = c["K"], c["T"], c["R"], c["RP"]
    ff, CW, nown, heads, span, width = c["ff"], c["CW"], c["nown"], c["heads"], c["span"], c["width"]
    NC = heads * (RP // 16)
    halves = RP // 16
    features = c["features"]
    me = lax.axis_index("kv")
    mt = lax.axis_index("tp")

    sends = []

    def guarded(limit, who, fn):
        if limit >= K:
            fn()
        else:
            pl.when(who < limit)(fn)

    def kv_copy(phase, src, dst, j):
        return pltpu.make_async_remote_copy(
            src_ref=src, dst_ref=dst, send_sem=kv_send.at[phase, j], recv_sem=kv_recv.at[phase, me],
            device_id={"kv": j}, device_id_type=MESH)

    def kv_wait(phase, dst, s):
        pltpu.make_async_remote_copy(
            src_ref=dst, dst_ref=dst, send_sem=kv_send.at[phase, s], recv_sem=kv_recv.at[phase, s],
            device_id={"kv": s}, device_id_type=MESH).wait_recv()

    def tp_copy(phase, src, dst, j):
        return pltpu.make_async_remote_copy(
            src_ref=src, dst_ref=dst, send_sem=tp_send.at[phase, j], recv_sem=tp_recv.at[phase, mt],
            device_id={"tp": j}, device_id_type=MESH)

    def tp_wait(phase, dst, s):
        pltpu.make_async_remote_copy(
            src_ref=dst, dst_ref=dst, send_sem=tp_send.at[phase, s], recv_sem=tp_recv.at[phase, s],
            device_id={"tp": s}, device_id_type=MESH).wait_recv()

    def kv_peer(i):
        return lax.rem(me + i, K)

    def tp_peer(i):
        return lax.rem(mt + i, T)

    count = [0]

    def load(src, dst):
        cp = pltpu.make_async_copy(src, dst, ld_sem.at[count[0]])
        count[0] += 1
        cp.start()
        return cp

    def load_cols(src, dst):
        n = src.shape[0]
        step = n // 4 if n % 64 == 0 else n
        return [load(src.at[pl.ds(r, step), :], dst.at[pl.ds(r, step), pl.ds(0, ff)]) for r in range(0, n, step)]

    def load_rows(src, dst):
        step = ff // 2 if ff % 32 == 0 else ff
        return [load(src.at[pl.ds(r, step), :], dst.at[pl.ds(r, step), :]) for r in range(0, ff, step)]

    def load_seqs(src, dst):
        step = 7 if R % 7 == 0 else R
        return [load(src.at[pl.ds(r, step)], dst.at[pl.ds(r, step)]) for r in range(0, R, step)]

    def wait_all(cps):
        for cp in cps:
            cp.wait()

    in1 = load_cols(wg1, wg1_v) + load_cols(wu1, wu1_v)

    barrier = pltpu.get_barrier_semaphore()
    for i in range(1, K):
        pl.semaphore_signal(barrier, inc=1, device_id={"kv": kv_peer(i)}, device_id_type=MESH)
    for i in range(1, T):
        pl.semaphore_signal(barrier, inc=1, device_id={"tp": tp_peer(i)}, device_id_type=MESH)

    down1 = load_rows(wd1, wd1_v)

    if nown * CW > ff:
        for w in (wg1_v, wu1_v, wg2_v, wu2_v):
            w[:, ff:] = jnp.zeros((w.shape[0], nown * CW - ff), BF16)
        for w in (wd1_v, wd2_v):
            w[ff:, :] = jnp.zeros((nown * CW - ff, w.shape[1]), BF16)

    xg_pad = jnp.zeros((RP - R, hid.shape[1]), BF16)
    xg[mt] = jnp.concatenate([hid[...], xg_pad], axis=0)

    pl.semaphore_wait(barrier, K - 1 + T - 1)

    if c["gathered"]:
        x = xg[mt]
    else:
        for i in range(1, T):
            cp = tp_copy(GATHER, xg.at[mt], xg.at[mt], tp_peer(i))
            cp.start()
            sends.append((None, None, cp))

    slot_all = c["head_total"]
    pick_row = lax.broadcasted_iota(jnp.int32, (slot_all, width), 0)
    pick_head = mt * heads + lax.broadcasted_iota(jnp.int32, (slot_all, width), 1) // HEAD_DIM
    fwx[...] = dot(fw[...], jnp.where(pick_row == pick_head, 1.0, 0.0).astype(BF16)).astype(BF16)

    place = me * span + lax.broadcasted_iota(jnp.int32, (SUB, span), 1)
    gpad[...] = jnp.zeros_like(gpad)
    for b in range(R):
        live = place[0:heads] < lens[b]
        gpad[b * SUB : b * SUB + heads, :] = jnp.where(live, cg[b], 0.0)
    kept = gpad[...]
    later = jnp.where(
        lax.broadcasted_iota(jnp.int32, (span, span), 0) > lax.broadcasted_iota(jnp.int32, (span, span), 1), 1.0, 0.0
    ).astype(BF16)
    top16 = kept.astype(BF16)
    rest = kept - top16.astype(F32)
    mid16 = rest.astype(BF16)
    low16 = (rest - mid16.astype(F32)).astype(BF16)
    after = dot(top16, later) + dot(mid16, later) + dot(low16, later)
    bias[...] = after
    total[...] = jnp.broadcast_to(after[:, 0:1] + kept[:, 0:1], total.shape)
    sc[...] = jnp.full_like(sc, FLOOR)
    pv[...] = jnp.zeros_like(pv)

    if not c["gathered"]:
        for i in range(1, T):
            tp_wait(GATHER, xg.at[tp_peer(i)], tp_peer(i))
        x = jnp.concatenate([xg[t] for t in range(T)], axis=1)

    def scaled_rows(x, gain):
        x32 = x.astype(F32)
        return (x32 * gain[...]).astype(BF16), jnp.sum(x32 * x32, axis=1, keepdims=True)

    def feed_forward(x, gain, loads, wg_v, wu_v, down, wd_v, rs_send, rs_recv, hbuf, rs, ag, extra):
        scaled, squares = scaled_rows(x, gain)
        square_tile = hi_lo(squares, RP)
        wait_all(loads)

        def part(j, dst):
            cols = pl.ds(pl.multiple_of(j * CW, LANES), CW)
            dst[:, 0:CW] = dot(scaled, wg_v[:, cols]).astype(BF16)
            dst[:, CW : 2 * CW] = dot(scaled, wu_v[:, cols]).astype(BF16)
            dst[:, 2 * CW :] = square_tile

        for i in range(1, K):
            j = kv_peer(i)

            def one(j=j):
                part(j, rs_send.at[j])
                kv_copy(rs, rs_send.at[j], rs_recv.at[me], j).start()

            guarded(nown, j, one)
            sends.append((nown, j, kv_copy(rs, rs_send.at[j], rs_recv.at[me], j)))

        guarded(nown, me, lambda: part(me, rs_recv.at[me]))
        more = extra()

        def own():
            tot = rs_recv[me].astype(F32)
            for i in range(1, K):
                s = kv_peer(i)
                kv_wait(rs, rs_recv.at[s], s)
                tot = tot + rs_recv[s].astype(F32)
            rscale = lax.rsqrt(from_hi_lo(tot[:, 2 * CW :]) / features + EPS)
            gate = tot[:, 0:CW] * rscale
            hbuf[me] = (gate / (1.0 + jnp.exp(-gate)) * (tot[:, CW : 2 * CW] * rscale)).astype(BF16)
            for i in range(1, K):
                kv_copy(ag, hbuf.at[me], hbuf.at[me], kv_peer(i)).start()

        guarded(nown, me, own)
        for i in range(1, K):
            sends.append((nown, me, kv_copy(ag, hbuf.at[me], hbuf.at[me], kv_peer(i))))
        wait_all(down)
        if nown == K:
            acc = dot(hbuf[me], wd_v[pl.ds(pl.multiple_of(me * CW, LANES), CW), :])
            for i in range(1, K):
                s = kv_peer(i)
                kv_wait(ag, hbuf.at[s], s)
                acc = acc + dot(hbuf[s], wd_v[pl.ds(pl.multiple_of(s * CW, LANES), CW), :])
        else:
            acc = jnp.zeros((RP, wd_v.shape[1]), F32)
            for s in range(nown):
                pl.when(me != s)(functools.partial(kv_wait, ag, hbuf.at[s], s))
                acc = acc + dot(hbuf[s], wd_v[s * CW : (s + 1) * CW, :])
        return acc, more

    def tp_sum(phase, acc, send, buf):
        send[...] = acc.astype(BF16)
        for i in range(1, T):
            cp = tp_copy(phase, send, buf.at[mt], tp_peer(i))
            cp.start()
            sends.append((None, None, cp))
        buf[mt] = send[...]
        for i in range(1, T):
            tp_wait(phase, buf.at[tp_peer(i)], tp_peer(i))
        tot = buf[0].astype(F32)
        for t in range(1, T):
            tot = tot + buf[t].astype(F32)
        return tot

    def rest_of_loads():
        proj = [load(wq, wq_v), load(wk, wk_v), load(wv, wv_v)]
        keys = load_seqs(ck, ck_v)
        values = load_seqs(cv, cv_v)
        proj_out = [load(wo, wo_v)]
        in2 = load_cols(wg2, wg2_v) + load_cols(wu2, wu2_v)
        down2 = load_rows(wd2, wd2_v)
        return proj, keys, values, proj_out, in2, down2

    acc, (proj, keys, values, proj_out, in2, down2) = feed_forward(
        x, g1, in1, wg1_v, wu1_v, down1, wd1_v, rs_send1, rs_recv1, hid1, RS1, AG1, rest_of_loads)
    x = (x.astype(F32) + 0.5 * tp_sum(SUM1, acc, sum1_send, sum1)).astype(BF16)

    scaled, squares = scaled_rows(x, gm)
    wait_all(proj)
    pq, pk, pvv, plog = dot(scaled, wq_v[...]), dot(scaled, wk_v[...]), dot(scaled, wv_v[...]), dot(scaled, fwx[...])
    square_tile = hi_lo(squares, RP)
    for n in range(NC):
        h, half = n // halves, n % halves
        r, l = slice(half * 16, half * 16 + 16), slice(h * HEAD_DIM, (h + 1) * HEAD_DIM)
        q_send[n, 0] = pq[r, l].astype(BF16)
        q_send[n, 1] = pk[r, l].astype(BF16)
        q_send[n, 2] = pvv[r, l].astype(BF16)
        q_send[n, 3] = hi_lo(plog[r, h * HEAD_DIM : h * HEAD_DIM + 1], 16)
        q_send[n, 4] = square_tile[r]

    def to_owners(phase, send, recv):
        for i in range(1, K):
            j = kv_peer(i)
            cp = kv_copy(phase, send.at[j], recv.at[me], j)
            guarded(NC, j, cp.start)
            sends.append((NC, j, cp))

    def gather_chunks(phase, buf):
        for n in range(NC):
            pl.when(me != n)(functools.partial(kv_wait, phase, buf.at[n], n))

    to_owners(RSQ, q_send, q_recv)
    factor = HEAD_DIM ** (-0.5)
    my_head = mt * heads + lax.rem(me, NC) // halves
    mine = lax.rem(me, NC)

    def own_query():
        q_recv[me] = q_send[mine]
        tot = [q_recv[me, p].astype(F32) for p in range(5)]
        for i in range(1, K):
            s = kv_peer(i)
            kv_wait(RSQ, q_recv.at[s], s)
            tot = [t + q_recv[s, p].astype(F32) for p, t in enumerate(tot)]
        rscale = lax.rsqrt(from_hi_lo(tot[4]) / features + EPS)
        query = (tot[0] * rscale).astype(BF16)
        q_buf[mine] = query
        for i in range(1, K):
            kv_copy(AGQ, q_buf.at[mine], q_buf.at[mine], kv_peer(i)).start()
        q32 = query.astype(F32)
        k32 = (tot[1] * rscale).astype(BF16).astype(F32)
        v32 = (tot[2] * rscale).astype(BF16).astype(F32)
        logit = from_hi_lo(tot[3]) * rscale + fb[my_head]
        rows[0] = jnp.broadcast_to(jnp.sum(q32 * k32, axis=1, keepdims=True) * factor, (16, LANES))
        rows[1] = v32
        rows[2] = jnp.broadcast_to(
            jnp.minimum(logit, 0.0) - jnp.log(1.0 + jnp.exp(-jnp.abs(logit))), (16, LANES))

    guarded(NC, me, own_query)
    for i in range(1, K):
        sends.append((NC, me, kv_copy(AGQ, q_buf.at[mine], q_buf.at[mine], kv_peer(i))))
    wait_all(keys)
    gather_chunks(AGQ, q_buf)
    for n in range(NC):
        h, half = n // halves, n % halves
        q_all[half * 16 : half * 16 + 16, h * HEAD_DIM : (h + 1) * HEAD_DIM] = q_buf[n].astype(F32)

    sel = lax.broadcasted_iota(jnp.int32, (SUB, width), 0) == lax.broadcasted_iota(jnp.int32, (SUB, width), 1) // HEAD_DIM
    for b in range(R):
        qb = jnp.where(sel, jnp.broadcast_to(q_all[b : b + 1, :], (SUB, width)), 0.0).astype(BF16)
        s = lax.dot_general(qb, ck_v[b], (((1,), (1,)), ((), ())), preferred_element_type=F32)
        s = s * factor + bias[b * SUB : (b + 1) * SUB, :]
        sc[b * SUB : (b + 1) * SUB, :] = jnp.where(place < lens[b], s, FLOOR)
    s = sc[...]
    top = jnp.max(s, axis=1, keepdims=True)
    weights = jnp.where(s > 0.5 * FLOOR, jnp.exp(s - top), 0.0)
    mass = jnp.sum(weights, axis=1, keepdims=True)
    sc[...] = weights
    lane = lax.broadcasted_iota(jnp.int32, stat.shape, 1)
    stat[...] = jnp.where(lane < 32, top, jnp.where(lane < 64, mass, total[...]))
    wait_all(values)
    for b in range(R):
        part = dot(sc[b * SUB : (b + 1) * SUB, :].astype(BF16), cv_v[b])
        for h in range(heads):
            pv[h, b * SUB : (b + 1) * SUB, :] = part[:, h * HEAD_DIM : (h + 1) * HEAD_DIM]
    for n in range(NC):
        h, half = n // halves, n % halves
        picked = pl.ds(half * 16 * SUB + h, 16, stride=SUB)
        a_send[n, 0] = pv.at[h][picked, :]
        a_send[n, 1] = stat[picked, :]

    to_owners(RSA, a_send, a_recv)

    def own_attended():
        a_recv[me] = a_send[mine]
        for i in range(1, K):
            kv_wait(RSA, a_recv.at[kv_peer(i)], kv_peer(i))
        own_score, fresh_value, fresh_gate = rows[0], rows[1], rows[2]
        ahead = fresh_gate
        tops = [None] * K
        for s in reversed(range(K)):
            st = a_recv[s, 1]
            tops[s] = st[:, 0:1] + ahead
            ahead = ahead + st[:, 64:65]
        peak = own_score
        for s in range(K):
            peak = jnp.maximum(peak, tops[s])
        fresh = jnp.exp(own_score - peak)
        num, den = fresh * fresh_value, fresh
        for s in range(K):
            keep = jnp.exp(tops[s] - peak)
            num = num + keep * a_recv[s, 0]
            den = den + keep * a_recv[s, 1][:, 32:33]
        att[mine] = (num / den).astype(BF16)
        for i in range(1, K):
            kv_copy(AGA, att.at[mine], att.at[mine], kv_peer(i)).start()

    guarded(NC, me, own_attended)
    for i in range(1, K):
        sends.append((NC, me, kv_copy(AGA, att.at[mine], att.at[mine], kv_peer(i))))
    wait_all(proj_out)
    gather_chunks(AGA, att)
    for n in range(NC):
        h, half = n // halves, n % halves
        att_all[half * 16 : half * 16 + 16, h * HEAD_DIM : (h + 1) * HEAD_DIM] = att[n]
    acc = dot(att_all[...], wo_v[...])
    x = (x.astype(F32) + tp_sum(SUM2, acc, sum2_send, sum2)).astype(BF16)

    acc, _ = feed_forward(
        x, g2, in2, wg2_v, wu2_v, down2, wd2_v, rs_send2, rs_recv2, hid2, RS2, AG2, lambda: None)

    if c["gathered"]:
        tot = tp_sum(SUM3, acc, fin_send, fin_recv)
        out[...] = (x.astype(F32) + 0.5 * tot).astype(BF16)[0:R]
    else:
        cols = hid.shape[1]
        for t in range(T):
            fin_send[t] = acc[:, t * cols : (t + 1) * cols]
            fin_x[t] = x[:, t * cols : (t + 1) * cols]
        for i in range(1, T):
            cp = tp_copy(SUM3, fin_send.at[tp_peer(i)], fin_recv.at[mt], tp_peer(i))
            cp.start()
            sends.append((None, None, cp))
        fin_recv[mt] = fin_send[mt]
        for i in range(1, T):
            tp_wait(SUM3, fin_recv.at[tp_peer(i)], tp_peer(i))
        tot = fin_recv[0]
        for t in range(1, T):
            tot = tot + fin_recv[t]
        out[...] = (fin_x[mt].astype(F32) + 0.5 * tot).astype(BF16)[0:R]

    for limit, who, cp in sends:
        if limit is None:
            cp.wait_send()
        else:
            guarded(limit, who, cp.wait_send)


def local(
    K, T,
    hidden_rows, first_gain, first_gate, first_up, first_down, mix_gain,
    query_weight, key_weight, value_weight, forget_weight, forget_bias, out_weight,
    second_gain, second_gate, second_up, second_down,
    cache_keys, cache_values, cache_gates, lengths,
):
    R, cols = hidden_rows.shape
    Dl = first_gate.shape[0]
    gathered = cols % LANES != 0
    RP = up_to(R, 16)
    width = query_weight.shape[1]
    heads = width // HEAD_DIM
    span = cache_keys.shape[1]
    ff = up_to(first_gate.shape[1], LANES)
    short = ff - first_gate.shape[1]
    if short:
        first_gate, first_up, second_gate, second_up = (
            jnp.pad(w, ((0, 0), (0, short))) for w in (first_gate, first_up, second_gate, second_up))
        first_down, second_down = (jnp.pad(w, ((0, short), (0, 0))) for w in (first_down, second_down))
    tiles = ff // LANES
    CW = up_to(tiles, K) // K * LANES
    nown = -(-ff // CW)
    ffc = nown * CW
    NC = heads * (RP // 16)
    assert NC <= K and heads <= SUB
    rows_in = lax.all_gather(hidden_rows, "tp", axis=1, tiled=True) if gathered else hidden_rows
    c = dict(K=K, T=T, R=R, RP=RP, ff=ff, CW=CW, nown=nown, heads=heads, span=span, width=width,
             features=Dl * K, gathered=gathered, head_total=forget_bias.shape[0])
    xc = rows_in.shape[1]
    vm = pltpu.VMEM
    msg = 2 * CW + LANES
    scratch = [
        vm((Dl, ffc), BF16), vm((Dl, ffc), BF16), vm((ffc, Dl), BF16),
        vm((Dl, width), BF16), vm((Dl, width), BF16), vm((Dl, width), BF16), vm((width, Dl), BF16),
        vm((Dl, ffc), BF16), vm((Dl, ffc), BF16), vm((ffc, Dl), BF16),
        vm((R, span, width), BF16), vm((R, span, width), BF16),
        vm((T, RP, xc), BF16), vm((K, RP, msg), BF16), vm((K, RP, msg), BF16), vm((K, RP, CW), BF16),
        vm((RP, Dl), BF16), vm((T, RP, Dl), BF16),
        vm((K, 5, 16, LANES), BF16), vm((K, 5, 16, LANES), BF16), vm((NC, 16, LANES), BF16), vm((RP, width), F32),
        vm((Dl, width), BF16), vm((RP * SUB, span), F32), vm((RP * SUB, span), F32), vm((RP * SUB, LANES), F32),
        vm((RP * SUB, span), F32), vm((heads, RP * SUB, LANES), F32), vm((RP * SUB, LANES), F32),
        vm((K, 2, 16, LANES), F32), vm((K, 2, 16, LANES), F32), vm((NC, 16, LANES), BF16), vm((RP, width), BF16),
        vm((RP, Dl), BF16), vm((T, RP, Dl), BF16),
        vm((K, RP, msg), BF16), vm((K, RP, msg), BF16), vm((K, RP, CW), BF16),
        vm((RP, Dl), BF16) if gathered else vm((T, RP, xc), F32),
        vm((T, RP, Dl), BF16) if gathered else vm((T, RP, xc), F32),
        vm((T, RP, xc), BF16), vm((3, 16, LANES), F32),
        pltpu.SemaphoreType.DMA((48,)),
        pltpu.SemaphoreType.DMA((8, K)), pltpu.SemaphoreType.DMA((8, K)),
        pltpu.SemaphoreType.DMA((4, T)), pltpu.SemaphoreType.DMA((4, T)),
    ]
    in_vmem = pl.BlockSpec(memory_space=pltpu.VMEM)
    in_smem = pl.BlockSpec(memory_space=pltpu.SMEM)
    anywhere = pl.BlockSpec(memory_space=pl.ANY)
    result = pl.pallas_call(
        functools.partial(kernel, c),
        out_shape=jax.ShapeDtypeStruct((R, xc), BF16),
        in_specs=[in_vmem] * 6 + [in_smem] * 2 + [anywhere] * 12,
        out_specs=in_vmem,
        scratch_shapes=scratch,
        compiler_params=pltpu.CompilerParams(
            collective_id=0, has_side_effects=True, vmem_limit_bytes=60 * 1024 * 1024),
        name="layer",
    )(
        rows_in, first_gain.reshape(1, Dl), mix_gain.reshape(1, Dl), second_gain.reshape(1, Dl),
        forget_weight, cache_gates, forget_bias, lengths,
        first_gate, first_up, first_down, query_weight, key_weight, value_weight, out_weight,
        second_gate, second_up, second_down, cache_keys, cache_values,
    )
    if gathered:
        return lax.dynamic_slice_in_dim(result, lax.axis_index("tp") * cols, cols, 1)
    return result


def solution(mesh):
    return jax.shard_map(
        functools.partial(local, mesh.shape["kv"], mesh.shape["tp"]),
        mesh=mesh,
        in_specs=(
            P(None, ("kv", "tp")),
            P("kv"),
            P("kv", "tp"),
            P("kv", "tp"),
            P("tp", "kv"),
            P("kv"),
            P("kv", "tp"),
            P("kv", "tp"),
            P("kv", "tp"),
            P("kv", None),
            P(),
            P("tp", "kv"),
            P("kv"),
            P("kv", "tp"),
            P("kv", "tp"),
            P("tp", "kv"),
            P(None, "kv", "tp"),
            P(None, "kv", "tp"),
            P(None, "tp", "kv"),
            P(),
        ),
        out_specs=P(None, ("kv", "tp")),
        check_vma=False,
    )
```

time: 401 us -> 88.1 us (0.22)
  blocking collectives: 192 us -> 0 us
  waiting for transfers between devices: 135 us -> 0 us
  Pallas kernels: 0 us -> 85 us
  matrix products: 29.2 us -> 0 us
  other arithmetic: 14.4 us -> 0 us
  between operations: 13.4 us -> 0.01 us
  local copies, waits for them, and re-layouts: 15.8 us -> 2.75 us
    psum x3 -> x0, waiting for transfers between devices: 135 us -> none  [the longest x2 74.3 us: feed_forward(): gate, up_act, squares = lax.psum((gate, up_act, squares), 'kv')]
    all_gather x5 -> x0, blocking collectives: 122 us -> none  [the longest x3 83.5 us: joined(): pieces = jax.tree.map(lambda part: lax.all_gather(part, axis), value)]
    pallas_call x0 -> x1, Pallas kernels: none -> 85 us  [local(): pl.pallas_call(functools.partial(kernel, c), out_shape=jax.ShapeDtypeStru...]
    psum x5 -> x0, blocking collectives: 70.8 us -> none  [the longest x2 38.8 us: feed_forward(): gate, up_act, squares = lax.psum((gate, up_act, squares), 'kv')]
    dot_general x13 -> x0, matrix products: 29.2 us -> none  [the longest x2 5.41 us: feed_forward(): return jnp.dot(hidden, w_down, preferred_element_type=jnp.float32)]
    reshape x6 -> x0, local copies, waits for them, and re-layouts: 10.6 us -> none  [the longest x1 10.4 us: attention(): keys = cache_keys.reshape(seqs, span, heads_dev, HEAD_DIM)]
    add x16 -> x0, other arithmetic: 6.4 us -> none  [the longest x7 4.92 us: join_parts(): mass_a * part_a + mass_b * part_b]
  transfers between devices with their start and end apart: 3 -> 0, of which waited for: 3 -> 0; matrix products, arithmetic and copies ran while one was open for 4% -> 0% of each run, Pallas kernels for 0% -> 0%
where the time goes in v1:
time: 88.1 us; the launch traced here: 87.8 us
  Pallas kernels  85 us (96%)
  local copies, waits for them, and re-layouts  2.75 us (3%)
    pallas_call x1, Pallas kernels, local(): pl.pallas_call(functools.partial(kernel, c), out_shape=jax.ShapeDtypeStru...  85 us
    unnamed x2, local copies, waits for them, and re-layouts  2.75 us

profile of v1, /device:TPU:0, one launch (start us, length us, event | category | flops | bytes accessed | tf_op | source)
XLA Modules:
  0.0 87.8 jit_solution(2184883329101949137)
XLA Ops:
  0.0 1.5 %copy.21.fw = bf16[512,16]{1,0:T(8,128)(2,1)} copy(bf16[512,16]{0,1:T(8,128)(2,1)} %param.29) | data formatting | bytes 32768 | tf_op args[9]
  1.5 85.0 %layer.1 = bf16[28,128]{1,0:T(8,128)(2,1)} custom-call(bf16[28,128]{1,0:T(8,128)(2,1)} %hid.1, f32[1,512]{1,0:T(1,128)} %bitcast.3, f32[1,512]{1,0:T(1,128)} %bitcast.4, f32[1,512]{1,0:T(1,128)} %bitcast.5, bf16[512,16]{1,0:T(8,128)(2,1)} %copy.21.fw, f32[28,4,256]{2,1,0:T(4,128)} %cg.1, f32[16]{0:T(128)} %fb.1, s32[28]{0:T(128)} %lens.1, ...), custom_call_target="tpu_custom_call" | custom-call | tf_op jit(solution)/shard_map/layer/pallas_call | solution.py:467
  86.5 1.3 %copy.23 = bf16[28,128]{1,0:T(8,128)(2,1)} copy(bf16[28,128]{1,0:T(8,128)(2,1)} %layer.1) | data formatting | bytes 14336

commit v2 on v1

--- a/solution.py
+++ b/solution.py
@@ -16,7 +16,7 @@
 F32 = jnp.float32
 BF16 = jnp.bfloat16
 
-RS1, AG1, RSQ, AGQ, RSA, AGA, RS2, AG2 = range(8)
+RS1, AG1, RSQ, AGQ, RSA, AGA, RS2, AG2, SQ1, SQM, SQ2, RSK, RSS = range(13)
 GATHER, SUM1, SUM2, SUM3 = range(4)
 
 
@@ -33,6 +33,19 @@
 
 def from_hi_lo(tile):
     return tile[:, 0:1] + tile[:, LANES // 2 : LANES // 2 + 1]
+
+
+def pack_column(column, parts):
+    lane = lax.broadcasted_iota(jnp.int32, (SUB, LANES), 1) // (LANES // parts)
+    tile = jnp.broadcast_to(column[0:SUB], (SUB, LANES))
+    for p in range(1, parts):
+        tile = jnp.where(lane == p, column[p * SUB : (p + 1) * SUB], tile)
+    return tile
+
+
+def unpack_column(tile, parts, offset=0):
+    step = LANES // parts
+    return jnp.concatenate([tile[:, p * step + offset : p * step + offset + 1] for p in range(parts)], axis=0)
 
 
 def dot(a, b):
@@ -46,7 +59,7 @@
     out,
     wg1_v, wu1_v, wd1_v, wq_v, wk_v, wv_v, wo_v, wg2_v, wu2_v, wd2_v, ck_v, cv_v,
     xg, rs_send1, rs_recv1, hid1, sum1_send, sum1,
-    q_send, q_recv, q_buf, q_all, fwx, gpad, bias, total, sc, pv, stat, a_send, a_recv, att, att_all,
+    sq_send, sq_recv, q_send, q_recv, k_send, k_recv, q_buf, q_all, fwx, gpad, bias, total, sc, pv, stat, a_send, a_recv, s_send, s_recv, att, att_all,
     sum2_send, sum2, rs_send2, rs_recv2, hid2, fin_send, fin_recv, fin_x, rows,
     ld_sem, kv_send, kv_recv, tp_send, tp_recv,
 ):
@@ -179,16 +192,34 @@
         x32 = x.astype(F32)
         return (x32 * gain[...]).astype(BF16), jnp.sum(x32 * x32, axis=1, keepdims=True)
 
-    def feed_forward(x, gain, loads, wg_v, wu_v, down, wd_v, rs_send, rs_recv, hbuf, rs, ag, extra):
+    parts = RP // SUB
+
+    def send_squares(n, phase, squares, limit):
+        sq_send[n] = pack_column(squares, parts)
+        for i in range(1, K):
+            j = kv_peer(i)
+            cp = kv_copy(phase, sq_send.at[n], sq_recv.at[n, me], j)
+            guarded(limit, j, cp.start)
+            sends.append((limit, j, cp))
+        sq_recv[n, me] = sq_send[n]
+
+    def row_scale(n, phase):
+        tot = sq_recv[n, me]
+        for i in range(1, K):
+            s = kv_peer(i)
+            kv_wait(phase, sq_recv.at[n, s], s)
+            tot = tot + sq_recv[n, s]
+        return lax.rsqrt(unpack_column(tot, parts) / features + EPS)
+
+    def feed_forward(n, sq, x, gain, loads, wg_v, wu_v, down, wd_v, rs_send, rs_recv, hbuf, rs, ag, extra):
         scaled, squares = scaled_rows(x, gain)
-        square_tile = hi_lo(squares, RP)
+        send_squares(n, sq, squares, nown)
         wait_all(loads)
 
         def part(j, dst):
             cols = pl.ds(pl.multiple_of(j * CW, LANES), CW)
             dst[:, 0:CW] = dot(scaled, wg_v[:, cols]).astype(BF16)
             dst[:, CW : 2 * CW] = dot(scaled, wu_v[:, cols]).astype(BF16)
-            dst[:, 2 * CW :] = square_tile
 
         for i in range(1, K):
             j = kv_peer(i)
@@ -204,12 +235,12 @@
         more = extra()
 
         def own():
+            rscale = row_scale(n, sq)
             tot = rs_recv[me].astype(F32)
             for i in range(1, K):
                 s = kv_peer(i)
                 kv_wait(rs, rs_recv.at[s], s)
                 tot = tot + rs_recv[s].astype(F32)
-            rscale = lax.rsqrt(from_hi_lo(tot[:, 2 * CW :]) / features + EPS)
             gate = tot[:, 0:CW] * rscale
             hbuf[me] = (gate / (1.0 + jnp.exp(-gate)) * (tot[:, CW : 2 * CW] * rscale)).astype(BF16)
             for i in range(1, K):
@@ -256,21 +287,16 @@
         return proj, keys, values, proj_out, in2, down2
 
     acc, (proj, keys, values, proj_out, in2, down2) = feed_forward(
-        x, g1, in1, wg1_v, wu1_v, down1, wd1_v, rs_send1, rs_recv1, hid1, RS1, AG1, rest_of_loads)
+        0, SQ1, x, g1, in1, wg1_v, wu1_v, down1, wd1_v, rs_send1, rs_recv1, hid1, RS1, AG1, rest_of_loads)
     x = (x.astype(F32) + 0.5 * tp_sum(SUM1, acc, sum1_send, sum1)).astype(BF16)
 
     scaled, squares = scaled_rows(x, gm)
+    send_squares(1, SQM, squares, NC)
     wait_all(proj)
-    pq, pk, pvv, plog = dot(scaled, wq_v[...]), dot(scaled, wk_v[...]), dot(scaled, wv_v[...]), dot(scaled, fwx[...])
-    square_tile = hi_lo(squares, RP)
+    pq = dot(scaled, wq_v[...])
     for n in range(NC):
         h, half = n // halves, n % halves
-        r, l = slice(half * 16, half * 16 + 16), slice(h * HEAD_DIM, (h + 1) * HEAD_DIM)
-        q_send[n, 0] = pq[r, l].astype(BF16)
-        q_send[n, 1] = pk[r, l].astype(BF16)
-        q_send[n, 2] = pvv[r, l].astype(BF16)
-        q_send[n, 3] = hi_lo(plog[r, h * HEAD_DIM : h * HEAD_DIM + 1], 16)
-        q_send[n, 4] = square_tile[r]
+        q_send[n] = pq[half * 16 : half * 16 + 16, h * HEAD_DIM : (h + 1) * HEAD_DIM].astype(BF16)
 
     def to_owners(phase, send, recv):
         for i in range(1, K):
@@ -284,30 +310,45 @@
             pl.when(me != n)(functools.partial(kv_wait, phase, buf.at[n], n))
 
     to_owners(RSQ, q_send, q_recv)
+    pk, pvv, plog = dot(scaled, wk_v[...]), dot(scaled, wv_v[...]), dot(scaled, fwx[...])
+    for n in range(NC):
+        h, half = n // halves, n % halves
+        r, l = slice(half * 16, half * 16 + 16), slice(h * HEAD_DIM, (h + 1) * HEAD_DIM)
+        k_send[n, 0] = pk[r, l].astype(BF16)
+        k_send[n, 1] = pvv[r, l].astype(BF16)
+        k_send[n, 2] = hi_lo(plog[r, h * HEAD_DIM : h * HEAD_DIM + 1], 16)
+    to_owners(RSK, k_send, k_recv)
     factor = HEAD_DIM ** (-0.5)
     my_head = mt * heads + lax.rem(me, NC) // halves
     mine = lax.rem(me, NC)
 
     def own_query():
-        q_recv[me] = q_send[mine]
-        tot = [q_recv[me, p].astype(F32) for p in range(5)]
+        rscale = row_scale(1, SQM)
+        first_half = jnp.broadcast_to(lax.rem(mine, halves) == 0, (16, 1))
+        rscale = jnp.where(first_half, rscale[0:16], rscale[RP - 16 : RP])
+        tot = q_send[mine].astype(F32)
         for i in range(1, K):
             s = kv_peer(i)
             kv_wait(RSQ, q_recv.at[s], s)
-            tot = [t + q_recv[s, p].astype(F32) for p, t in enumerate(tot)]
-        rscale = lax.rsqrt(from_hi_lo(tot[4]) / features + EPS)
-        query = (tot[0] * rscale).astype(BF16)
-        q_buf[mine] = query
+            tot = tot + q_recv[s].astype(F32)
+        q_buf[mine] = (tot * rscale).astype(BF16)
         for i in range(1, K):
             kv_copy(AGQ, q_buf.at[mine], q_buf.at[mine], kv_peer(i)).start()
-        q32 = query.astype(F32)
-        k32 = (tot[1] * rscale).astype(BF16).astype(F32)
-        v32 = (tot[2] * rscale).astype(BF16).astype(F32)
-        logit = from_hi_lo(tot[3]) * rscale + fb[my_head]
-        rows[0] = jnp.broadcast_to(jnp.sum(q32 * k32, axis=1, keepdims=True) * factor, (16, LANES))
-        rows[1] = v32
-        rows[2] = jnp.broadcast_to(
-            jnp.minimum(logit, 0.0) - jnp.log(1.0 + jnp.exp(-jnp.abs(logit))), (16, LANES))
+        rows[0] = jnp.broadcast_to(rscale, (16, LANES))
+
+    def own_fresh():
+        tot = [k_send[mine, p].astype(F32) for p in range(3)]
+        for i in range(1, K):
+            s = kv_peer(i)
+            kv_wait(RSK, k_recv.at[s], s)
+            tot = [t + k_recv[s, p].astype(F32) for p, t in enumerate(tot)]
+        rscale = rows[0]
+        q32 = q_buf[mine].astype(F32)
+        k32 = (tot[0] * rscale).astype(BF16).astype(F32)
+        v32 = (tot[1] * rscale).astype(BF16).astype(F32)
+        logit = from_hi_lo(tot[2]) * rscale + fb[my_head]
+        own_score = jnp.broadcast_to(jnp.sum(q32 * k32, axis=1, keepdims=True) * factor, (16, LANES))
+        return own_score, v32, jnp.minimum(logit, 0.0) - jnp.log(1.0 + jnp.exp(-jnp.abs(logit)))
 
     guarded(NC, me, own_query)
     for i in range(1, K):
@@ -330,7 +371,8 @@
     mass = jnp.sum(weights, axis=1, keepdims=True)
     sc[...] = weights
     lane = lax.broadcasted_iota(jnp.int32, stat.shape, 1)
-    stat[...] = jnp.where(lane < 32, top, jnp.where(lane < 64, mass, total[...]))
+    lane = lane % (LANES // 2)
+    stat[...] = jnp.where(lane < 16, top, jnp.where(lane < 32, mass, total[...]))
     wait_all(values)
     for b in range(R):
         part = dot(sc[b * SUB : (b + 1) * SUB, :].astype(BF16), cv_v[b])
@@ -339,22 +381,27 @@
     for n in range(NC):
         h, half = n // halves, n % halves
         picked = pl.ds(half * 16 * SUB + h, 16, stride=SUB)
-        a_send[n, 0] = pv.at[h][picked, :]
-        a_send[n, 1] = stat[picked, :]
-
+        a_send[n] = pv.at[h][picked, :].astype(BF16)
+        st = stat[picked, :]
+        left = lax.broadcasted_iota(jnp.int32, (SUB, LANES), 1) < LANES // 2
+        s_send[n] = jnp.where(left, st[0:SUB], st[SUB : 2 * SUB])
+
+    to_owners(RSS, s_send, s_recv)
     to_owners(RSA, a_send, a_recv)
 
     def own_attended():
+        own_score, fresh_value, fresh_gate = own_fresh()
         a_recv[me] = a_send[mine]
-        for i in range(1, K):
+        s_recv[me] = s_send[mine]
+        for i in range(1, K):
+            kv_wait(RSS, s_recv.at[kv_peer(i)], kv_peer(i))
             kv_wait(RSA, a_recv.at[kv_peer(i)], kv_peer(i))
-        own_score, fresh_value, fresh_gate = rows[0], rows[1], rows[2]
         ahead = fresh_gate
         tops = [None] * K
         for s in reversed(range(K)):
-            st = a_recv[s, 1]
-            tops[s] = st[:, 0:1] + ahead
-            ahead = ahead + st[:, 64:65]
+            st = s_recv[s]
+            tops[s] = unpack_column(st, 2) + ahead
+            ahead = ahead + unpack_column(st, 2, 32)
         peak = own_score
         for s in range(K):
             peak = jnp.maximum(peak, tops[s])
@@ -362,8 +409,8 @@
         num, den = fresh * fresh_value, fresh
         for s in range(K):
             keep = jnp.exp(tops[s] - peak)
-            num = num + keep * a_recv[s, 0]
-            den = den + keep * a_recv[s, 1][:, 32:33]
+            num = num + keep * a_recv[s].astype(F32)
+            den = den + keep * unpack_column(s_recv[s], 2, 16)
         att[mine] = (num / den).astype(BF16)
         for i in range(1, K):
             kv_copy(AGA, att.at[mine], att.at[mine], kv_peer(i)).start()
@@ -380,7 +427,7 @@
     x = (x.astype(F32) + tp_sum(SUM2, acc, sum2_send, sum2)).astype(BF16)
 
     acc, _ = feed_forward(
-        x, g2, in2, wg2_v, wu2_v, down2, wd2_v, rs_send2, rs_recv2, hid2, RS2, AG2, lambda: None)
+        2, SQ2, x, g2, in2, wg2_v, wu2_v, down2, wd2_v, rs_send2, rs_recv2, hid2, RS2, AG2, lambda: None)
 
     if c["gathered"]:
         tot = tp_sum(SUM3, acc, fin_send, fin_recv)
@@ -440,7 +487,7 @@
              features=Dl * K, gathered=gathered, head_total=forget_bias.shape[0])
     xc = rows_in.shape[1]
     vm = pltpu.VMEM
-    msg = 2 * CW + LANES
+    msg = 2 * CW
     scratch = [
         vm((Dl, ffc), BF16), vm((Dl, ffc), BF16), vm((ffc, Dl), BF16),
         vm((Dl, width), BF16), vm((Dl, width), BF16), vm((Dl, width), BF16), vm((width, Dl), BF16),
@@ -448,17 +495,20 @@
         vm((R, span, width), BF16), vm((R, span, width), BF16),
         vm((T, RP, xc), BF16), vm((K, RP, msg), BF16), vm((K, RP, msg), BF16), vm((K, RP, CW), BF16),
         vm((RP, Dl), BF16), vm((T, RP, Dl), BF16),
-        vm((K, 5, 16, LANES), BF16), vm((K, 5, 16, LANES), BF16), vm((NC, 16, LANES), BF16), vm((RP, width), F32),
+        vm((3, SUB, LANES), F32), vm((3, K, SUB, LANES), F32),
+        vm((K, 16, LANES), BF16), vm((K, 16, LANES), BF16),
+        vm((K, 3, 16, LANES), BF16), vm((K, 3, 16, LANES), BF16), vm((NC, 16, LANES), BF16), vm((RP, width), F32),
         vm((Dl, width), BF16), vm((RP * SUB, span), F32), vm((RP * SUB, span), F32), vm((RP * SUB, LANES), F32),
         vm((RP * SUB, span), F32), vm((heads, RP * SUB, LANES), F32), vm((RP * SUB, LANES), F32),
-        vm((K, 2, 16, LANES), F32), vm((K, 2, 16, LANES), F32), vm((NC, 16, LANES), BF16), vm((RP, width), BF16),
+        vm((K, 16, LANES), BF16), vm((K, 16, LANES), BF16),
+        vm((K, SUB, LANES), F32), vm((K, SUB, LANES), F32), vm((NC, 16, LANES), BF16), vm((RP, width), BF16),
         vm((RP, Dl), BF16), vm((T, RP, Dl), BF16),
         vm((K, RP, msg), BF16), vm((K, RP, msg), BF16), vm((K, RP, CW), BF16),
         vm((RP, Dl), BF16) if gathered else vm((T, RP, xc), F32),
         vm((T, RP, Dl), BF16) if gathered else vm((T, RP, xc), F32),
-        vm((T, RP, xc), BF16), vm((3, 16, LANES), F32),
+        vm((T, RP, xc), BF16), vm((1, 16, LANES), F32),
         pltpu.SemaphoreType.DMA((48,)),
-        pltpu.SemaphoreType.DMA((8, K)), pltpu.SemaphoreType.DMA((8, K)),
+        pltpu.SemaphoreType.DMA((13, K)), pltpu.SemaphoreType.DMA((13, K)),
         pltpu.SemaphoreType.DMA((4, T)), pltpu.SemaphoreType.DMA((4, T)),
     ]
     in_vmem = pl.BlockSpec(memory_space=pltpu.VMEM)

time: 88.1 us -> 82 us (0.931)
  Pallas kernels: 85 us -> 79 us
    pallas_call x1, Pallas kernels: 85 us -> 79 us  [local(): pl.pallas_call(functools.partial(kernel, c), out_shape=jax.ShapeDtypeStru...]
where the time goes in v2:
time: 82 us; the launch traced here: 81.7 us
  Pallas kernels  79 us (96%)
  local copies, waits for them, and re-layouts  2.75 us (3%)
    pallas_call x1, Pallas kernels, local(): pl.pallas_call(functools.partial(kernel, c), out_shape=jax.ShapeDtypeStru...  79 us
    unnamed x2, local copies, waits for them, and re-layouts  2.75 us

profile of v2, /device:TPU:0, one launch (start us, length us, event | category | flops | bytes accessed | tf_op | source)
XLA Modules:
  0.0 81.7 jit_solution(1222664603791396071)
XLA Ops:
  0.0 1.5 %copy.21.fw = bf16[512,16]{1,0:T(8,128)(2,1)} copy(bf16[512,16]{0,1:T(8,128)(2,1)} %param.29) | data formatting | bytes 32768 | tf_op args[9]
  1.5 79.0 %layer.1 = bf16[28,128]{1,0:T(8,128)(2,1)} custom-call(bf16[28,128]{1,0:T(8,128)(2,1)} %hid.1, f32[1,512]{1,0:T(1,128)} %bitcast.3, f32[1,512]{1,0:T(1,128)} %bitcast.4, f32[1,512]{1,0:T(1,128)} %bitcast.5, bf16[512,16]{1,0:T(8,128)(2,1)} %copy.21.fw, f32[28,4,256]{2,1,0:T(4,128)} %cg.1, f32[16]{0:T(128)} %fb.1, s32[28]{0:T(128)} %lens.1, ...), custom_call_target="tpu_custom_call" | custom-call | tf_op jit(solution)/shard_map/layer/pallas_call | solution.py:517
  80.4 1.3 %copy.23 = bf16[28,128]{1,0:T(8,128)(2,1)} copy(bf16[28,128]{1,0:T(8,128)(2,1)} %layer.1) | data formatting | bytes 14336
